TPU v7x, 32 devices: a whole 2x2x4 slice. The times are simulated.
32 devices in a mesh: fs: 4 (over y, x), tp: 8 (over z, core).
Axes of the slice: x: 2, y: 2, z: 4, core: 2. Of those that a mesh axis runs over, the one named last changes fastest.
Arguments:
- saved_input: bfloat16 [4096, 4096], P('fs', 'tp'), may hold values from -6 to 6
- query_cot: bfloat16 [4096, 4096], P('fs', 'tp'), may hold values from -6 to 6
- key_cot: bfloat16 [4096, 4096], P('fs', 'tp'), may hold values from -6 to 6
- query_master: float32 [4096, 4096], P('fs', 'tp'), may hold values from -0.09375 to 0.09375
- key_master: float32 [4096, 4096], P('fs', 'tp'), may hold values from -0.09375 to 0.09375
- query_basis: bfloat16 [4096, 256], P('fs'), may hold values from -3 to 3
- key_basis: bfloat16 [4096, 256], P('fs'), may hold values from -3 to 3
- query_first: float32 [256, 4096], P('fs', 'tp'), may hold values from -240 to 240
- query_second: float32 [256, 4096], P('fs', 'tp'), may hold values from 1000 to 20000
- key_first: float32 [256, 4096], P('fs', 'tp'), may hold values from -240 to 240
- key_second: float32 [256, 4096], P('fs', 'tp'), may hold values from 1000 to 20000
Outputs:
- query_step: float32 [4096, 4096], P('fs', 'tp')
- query_weight: float32 [4096, 4096], P('fs', 'tp')
- query_copy: bfloat16 [4096, 4096], P(None, 'tp')
- query_first_new: float32 [256, 4096], P('fs', 'tp')
- query_second_new: float32 [256, 4096], P('fs', 'tp')
- key_step: float32 [4096, 4096], P('fs', 'tp')
- key_weight: float32 [4096, 4096], P('fs', 'tp')
- key_copy: bfloat16 [4096, 4096], P(None, 'tp')
- key_first_new: float32 [256, 4096], P('fs', 'tp')
- key_second_new: float32 [256, 4096], P('fs', 'tp')
All inputs are finite; a program needn't handle non-finite values.
Results may differ from a plain program's by a relative error of at most 0.0065.
Values may be sent and summed in bfloat16 or wider, within the bound.
A program may use at most 64 MiB of HBM per device.

v0:
```python
import jax
import jax.numpy as jnp
from jax import lax
from jax.sharding import PartitionSpec as P

D = 4096
HD = 128


moment_decay = 0.8
square_decay = 0.9
square_floor = 1.0
norm_floor = 0.01
step_rate = 0.01


def split_product(low_part, cot_part):
    upper = low_part.astype(jnp.bfloat16)
    lower = (low_part - upper.astype(jnp.float32)).astype(jnp.bfloat16)
    return jnp.dot(upper.T, cot_part, preferred_element_type=jnp.float32) + jnp.dot(
        lower.T, cot_part, preferred_element_type=jnp.float32
    )


def cot_rows(query_low, key_low, cot_wide, width):

    def low_rows(start, count):
        return jnp.concatenate(
            [
                split_product(query_low, cot_wide[:, :width]),
                split_product(key_low, cot_wide[:, width:]),
            ],
            axis=1,
        )

    return low_rows


def head_squares(update):
    by_head = update.reshape(update.shape[0], -1, HD)
    return jnp.sum(by_head * by_head, axis=(0, 2))


def apply_scale(update, total):
    scale = 1.0 / jnp.sqrt(total / (D * HD) + norm_floor)
    by_head = update.reshape(update.shape[0], -1, HD)
    return (by_head * scale[None, :, None]).reshape(update.shape)


def body(
    saved_input,
    query_cot,
    key_cot,
    query_master,
    key_master,
    query_basis,
    key_basis,
    query_first,
    query_second,
    key_first,
    key_second,
):
    width = query_cot.shape[1]
    low_count = query_first.shape[0]
    cotangents = jnp.concatenate([query_cot, key_cot], axis=1)
    bases = (
        lax.all_gather(query_basis, "fs", axis=0, tiled=True),
        lax.all_gather(key_basis, "fs", axis=0, tiled=True),
    )
    columns = saved_input.shape[1]
    offset = lax.axis_index("tp") * columns
    query_part = lax.dynamic_slice_in_dim(bases[0], offset, columns, 0)
    key_part = lax.dynamic_slice_in_dim(bases[1], offset, columns, 0)
    both_part = jnp.concatenate([query_part, key_part], axis=1)
    local_low = jnp.dot(saved_input, both_part, preferred_element_type=jnp.float32)
    summed_low = lax.psum(local_low, "tp")
    rank = query_basis.shape[1]
    low_rows = cot_rows(summed_low[:, :rank], summed_low[:, rank:], cotangents, width)
    projected = lax.psum_scatter(
        low_rows(jnp.int32(0), lax.axis_size("fs") * low_count),
        "fs",
        scatter_dimension=0,
        tiled=True,
    )
    firsts = jnp.concatenate([query_first, key_first], axis=1)
    seconds = jnp.concatenate([query_second, key_second], axis=1)
    first_new = moment_decay * firsts + (1.0 - moment_decay) * projected
    second_new = square_decay * seconds + (1.0 - square_decay) * projected * projected
    ratio = (first_new / jnp.sqrt(second_new + square_floor)).astype(jnp.bfloat16)
    piece = lax.all_gather(ratio, "fs", axis=0, tiled=True)
    query_update = jnp.dot(query_basis, piece[:, :width], preferred_element_type=jnp.float32)
    key_update = jnp.dot(key_basis, piece[:, width:], preferred_element_type=jnp.float32)
    query_total, key_total = lax.psum((head_squares(query_update), head_squares(key_update)), "fs")
    query_step = apply_scale(query_update, query_total)
    key_step = apply_scale(key_update, key_total)
    query_weight = query_master - step_rate * query_step
    key_weight = key_master - step_rate * key_step
    copies = (
        lax.all_gather(query_weight.astype(jnp.bfloat16), "fs", axis=0, tiled=True),
        lax.all_gather(key_weight.astype(jnp.bfloat16), "fs", axis=0, tiled=True),
    )
    return (
        query_step,
        query_weight,
        copies[0],
        first_new[:, :width],
        second_new[:, :width],
        key_step,
        key_weight,
        copies[1],
        first_new[:, width:],
        second_new[:, width:],
    )


def solution(mesh):
    placed = (
        P("fs", "tp"),
        P("fs", "tp"),
        P("fs", "tp"),
        P("fs", "tp"),
        P("fs", "tp"),
        P("fs", None),
        P("fs", None),
        P("fs", "tp"),
        P("fs", "tp"),
        P("fs", "tp"),
        P("fs", "tp"),
    )
    return jax.shard_map(
        body,
        mesh=mesh,
        in_specs=placed,
        out_specs=(
            P("fs", "tp"),
            P("fs", "tp"),
            P(None, "tp"),
            P("fs", "tp"),
            P("fs", "tp"),
            P("fs", "tp"),
            P("fs", "tp"),
            P(None, "tp"),
            P("fs", "tp"),
            P("fs", "tp"),
        ),
        check_vma=False,
    )
```

profile of v0, /device:TPU:0, one launch (start us, length us, event | category | flops | bytes accessed | tf_op | source)
XLA Modules:
  0.0 337.9 jit_solution(4425682865284060865)
XLA Ops:
  7.2 0.0 all-gather.5.cloned.1.call-start
  7.2 0.7 all-gather.5.cloned.1.call-update
  7.9 0.0 all-gather.7.cloned.1.call-start
  8.0 0.7 all-gather.7.cloned.1.call-update
  8.7 0.0 all-reduce.3.cloned.1.call-start
  8.7 39.1 %all-gather.5.cloned.1.call-done = bf16[4096,256]{1,0:T(8,128)(2,1)} async-done(((bf16[1024,256]{1,0:T(8,128)(2,1)}), bf16[4096,256]{1,0:T(8,128)(2,1)}) %all-gather.5.cloned.1.call-update) | async-done | bytes 2097168 | tf_op jit(solution)/shard_map/all_gather | solution.py:67
  47.8 1.0 constant_dynamic-slice_fusion.1
  48.7 36.1 %all-gather.7.cloned.1.call-done = bf16[4096,256]{1,0:T(8,128)(2,1)} async-done(((bf16[1024,256]{1,0:T(8,128)(2,1)}), bf16[4096,256]{1,0:T(8,128)(2,1)}) %all-gather.7.cloned.1.call-update) | async-done | bytes 2097168 | tf_op jit(solution)/shard_map/all_gather | solution.py:68
  84.8 1.0 constant_dynamic-slice_fusion
  85.8 2.1 convolution_bitcast_fusion
  87.9 0.0 all-reduce.3.cloned.1.call-update
  87.9 0.0 reduce-scatter.2.cloned.1.call-start
  88.0 65.2 %all-reduce.3.cloned.1.call-done = f32[1024,512]{0,1:T(8,128)} async-done(((f32[1024,512]{0,1:T(8,128)}), f32[1024,512]{0,1:T(8,128)}) %all-reduce.3.cloned.1.call-update) | async-done | bytes 2097168 | tf_op jit(solution)/shard_map/psum | solution.py:76
  153.2 1.8 fusion.10
  155.0 0.1 copy-done.3
  155.1 0.4 convolution_add_fusion
  155.5 0.8 copy-done.5
  156.3 0.4 fusion.9
  156.7 0.4 convolution_add_fusion.1
  157.2 1.1 pad_maximum_fusion
  158.3 0.0 reduce-scatter.2.cloned.1.call-update
  158.3 0.0 all-gather.9.cloned.1.call-start
  158.4 27.6 %reduce-scatter.2.cloned.1.call-done = f32[64,1024]{1,0:T(8,128)} async-done(((f32[256,1024]{1,0:T(8,128)}), f32[64,1024]{1,0:T(8,128)}) %reduce-scatter.2.cloned.1.call-update) | async-done | bytes 262160 | tf_op jit(solution)/shard_map/reduce_scatter | solution.py:79
  186.0 1.8 multiply_convert_fusion
  187.8 10.2 %all_gather.17 = bf16[256,1024]{1,0:T(8,128)(2,1)S(1)} all-gather(bf16[64,1024]{1,0:T(8,128)(2,1)S(1)} %get-tuple-element.38), channel_id=1, replica_groups=mesh['fs'=4,'tp'=8] {'fs'}, dimensions={0}, use_global_device_ids=true | all-gather | bytes 655360 | tf_op jit(solution)/shard_map/all_gather | solution.py:90
  198.0 1.6 multiply_reduce_fusion
  199.6 1.8 multiply_reduce_fusion.1
  201.4 0.1 bitcast_reduce_fusion
  201.5 0.1 bitcast_reduce_fusion.1
  201.6 2.9 copy.29
  204.5 8.9 %all-reduce = (f32[4]{0:T(128)S(1)}, f32[4]{0:T(128)S(1)}) all-reduce(f32[4]{0:T(128)S(1)} %bitcast_reduce_fusion.1, f32[4]{0:T(128)S(1)} %bitcast_reduce_fusion), channel_id=1, replica_groups=mesh['fs'=4,'tp'=8] {'fs'}, use_global_device_ids=true, to_apply=%region_4.0 | all-reduce | flops 8 | bytes 64 | tf_op jit(solution)/shard_map/psum | solution.py:93
  213.4 0.1 broadcast_bitcast_fusion.1
  213.5 5.0 %fusion.13 = (bf16[1024,512]{0,1:T(8,128)(2,1)}, f32[1024,512]{0,1:T(8,128)}, f32[1024,512]{0,1:T(8,128)}) fusion(f32[1024,512]{0,1:T(8,128)} %copy.29, f32[512,1024]{1,0:T(8,128)} %get-tuple-element.46, f32[512]{0:T(512)S(1)} %broadcast_bitcast_fusion.1), kind=kLoop, calls=%fused_computation.39 | loop fusion | flops 2097152 | bytes 9439232 | tf_op jit(solution)/shard_map/convert_element_type | solution.py:99
  218.5 0.0 all-gather.9.cloned.1.call-update
  218.5 0.0 all-gather.11.cloned.1.call-start
  218.5 2.9 copy.30
  221.4 0.1 broadcast_bitcast_fusion
  221.5 4.4 %fusion.12 = (bf16[1024,512]{0,1:T(8,128)(2,1)}, f32[1024,512]{0,1:T(8,128)}, f32[1024,512]{0,1:T(8,128)}) fusion(f32[1024,512]{0,1:T(8,128)} %copy.30, f32[512,1024]{1,0:T(8,128)S(1)} %get-tuple-element.48, f32[512]{0:T(512)S(1)} %broadcast_bitcast_fusion), kind=kLoop, calls=%fused_computation.38 | loop fusion | flops 2097152 | bytes 9439232 | tf_op jit(solution)/shard_map/convert_element_type | solution.py:100
  225.9 0.0 all-gather.11.cloned.1.call-update
  226.0 3.3 copy.35
  229.3 1.8 copy.34
  231.1 3.0 copy.32
  234.1 1.8 copy.31
  235.9 1.8 fusion.16
  237.7 32.7 %all-gather.9.cloned.1.call-done = bf16[4096,512]{0,1:T(8,128)(2,1)} async-done(((bf16[1024,512]{0,1:T(8,128)(2,1)}), bf16[4096,512]{0,1:T(8,128)(2,1)}) %all-gather.9.cloned.1.call-update) | async-done | bytes 4194320 | tf_op jit(solution)/shard_map/all_gather | solution.py:99
  270.3 6.4 %copy.33 = bf16[4096,512]{1,0:T(8,128)(2,1)} copy(bf16[4096,512]{0,1:T(8,128)(2,1)} %all-gather.9.cloned.1.call-done) | data formatting | bytes 8388608
  276.7 47.9 %all-gather.11.cloned.1.call-done = bf16[4096,512]{0,1:T(8,128)(2,1)} async-done(((bf16[1024,512]{0,1:T(8,128)(2,1)}), bf16[4096,512]{0,1:T(8,128)(2,1)}) %all-gather.11.cloned.1.call-update) | async-done | bytes 4194320 | tf_op jit(solution)/shard_map/all_gather | solution.py:100
  324.6 6.4 %copy.36 = bf16[4096,512]{1,0:T(8,128)(2,1)} copy(bf16[4096,512]{0,1:T(8,128)(2,1)} %all-gather.11.cloned.1.call-done) | data formatting | bytes 8388608
  (21 shorter events, 0.1 us)
Async XLA Ops:
  7.2 78.6 %copy-start = (bf16[1024,512]{1,0:T(8,128)(2,1)S(1)}, bf16[1024,512]{1,0:T(8,128)(2,1)}, u32[]{:S(2)}) copy-start(bf16[1024,512]{1,0:T(8,128)(2,1)} %param.11) | copy-start | bytes 3145732
  7.2 40.6 %all-gather.5.cloned.1.call-start = ((), (), s32[]{:S(2)}) async-start(), calls=%async_computation.1 | async-start | bytes 2621440 | tf_op jit(solution)/shard_map/all_gather | solution.py:67
  7.9 76.9 %all-gather.7.cloned.1.call-start = ((), (), s32[]{:S(2)}) async-start(), calls=%async_computation.2 | async-start | bytes 2621440 | tf_op jit(solution)/shard_map/all_gather | solution.py:68
  8.7 144.5 %all-reduce.3.cloned.1.call-start = ((), (), s32[]{:S(2)}) async-start(), calls=%async_computation.3 | async-start | bytes 4194304 | tf_op jit(solution)/shard_map/psum | solution.py:76
  85.8 67.4 %copy-start.4 = (bf16[1024,512]{1,0:T(8,128)(2,1)S(1)}, bf16[1024,512]{1,0:T(8,128)(2,1)}, u32[]{:S(2)}) copy-start(bf16[1024,512]{1,0:T(8,128)(2,1)} %param.13) | copy-start | bytes 3145732
  87.9 98.1 %reduce-scatter.2.cloned.1.call-start = ((), (), s32[]{:S(2)}) async-start(), calls=%async_computation.4 | async-start | bytes 1310720 | tf_op jit(solution)/shard_map/reduce_scatter | solution.py:79
  153.2 1.9 copy-start.3
  155.1 1.2 copy-start.5
  157.2 28.8 %copy-start.7 = (f32[64,512]{1,0:T(8,128)S(1)}, f32[64,512]{1,0:T(8,128)}, u32[]{:S(2)}) copy-start(f32[64,512]{1,0:T(8,128)} %param.21) | copy-start | bytes 393220
  157.2 28.8 %copy-start.8 = (f32[64,512]{1,0:T(8,128)S(1)}, f32[64,512]{1,0:T(8,128)}, u32[]{:S(2)}) copy-start(f32[64,512]{1,0:T(8,128)} %param.19) | copy-start | bytes 393220
  157.2 28.8 %copy-start.9 = (f32[64,512]{1,0:T(8,128)S(1)}, f32[64,512]{1,0:T(8,128)}, u32[]{:S(2)}) copy-start(f32[64,512]{1,0:T(8,128)} %param.20) | copy-start | bytes 393220
  157.2 28.8 %copy-start.10 = (f32[64,512]{1,0:T(8,128)S(1)}, f32[64,512]{1,0:T(8,128)}, u32[]{:S(2)}) copy-start(f32[64,512]{1,0:T(8,128)} %param.18) | copy-start | bytes 393220
  158.3 112.0 %all-gather.9.cloned.1.call-start = ((), (), s32[]{:S(2)}) async-start(), calls=%async_computation.5 | async-start | bytes 5242880 | tf_op jit(solution)/shard_map/all_gather | solution.py:99
  187.8 11.8 %copy-start.6 = (bf16[1024,256]{1,0:T(8,128)(2,1)S(1)}, bf16[1024,256]{1,0:T(8,128)(2,1)}, u32[]{:S(2)}) copy-start(bf16[1024,256]{1,0:T(8,128)(2,1)} %param.16) | copy-start | bytes 1572868
  218.5 106.2 %all-gather.11.cloned.1.call-start = ((), (), s32[]{:S(2)}) async-start(), calls=%async_computation.6 | async-start | bytes 5242880 | tf_op jit(solution)/shard_map/all_gather | solution.py:100
  226.0 3.3 copy-start.2
  231.1 3.0 copy-start.1
Sparse Core Ops, SparseCore 0:
  9.8 37.8 all-gather.4
  49.6 35.1 all-gather.6
  88.0 65.0 all-reduce.2
  158.4 27.5 reduce-scatter.1
  218.6 51.6 all-gather.8
  272.0 52.5 all-gather.10
where the time goes:
time: 339 us; the launch traced here: 338 us
  waiting for transfers between devices  250 us (74%)
  local copies, waits for them, and re-layouts  33.3 us (10%)
  blocking collectives  19.1 us (6%)
  between operations  14.2 us (4%)
  other arithmetic  12.5 us (4%)
  matrix products  8.61 us (3%)
    psum x1, waiting for transfers between devices, body(): summed_low = lax.psum(local_low, 'tp')  65.2 us
    all_gather x1, waiting for transfers between devices, body(): lax.all_gather(key_weight.astype(jnp.bfloat16), 'fs', axis=0, tiled=True)  47.9 us
    all_gather x1, waiting for transfers between devices, body(): lax.all_gather(query_basis, 'fs', axis=0, tiled=True)  39.1 us
    all_gather x1, waiting for transfers between devices, body(): lax.all_gather(key_basis, 'fs', axis=0, tiled=True)  36.1 us
    all_gather x1, waiting for transfers between devices, body(): lax.all_gather(query_weight.astype(jnp.bfloat16), 'fs', axis=0, tiled=True)  32.7 us
    unnamed x30, local copies, waits for them, and re-layouts  29.4 us
    reduce_scatter x1, waiting for transfers between devices, body(): lax.psum_scatter(low_rows(jnp.int32(0), lax.axis_size('fs') * low_count),...  27.6 us
    all_gather x1, blocking collectives, body(): piece = lax.all_gather(ratio, 'fs', axis=0, tiled=True)  10.2 us
  transfers between devices with their start and end apart: 6, of which 6 were waited for; matrix products, arithmetic and copies ran while one was open for 8% of the time, Pallas kernels for 0%

commit v1 on v0

v1 whole, which is shorter than its diff:
```python
import functools

import jax
import jax.numpy as jnp
from jax import lax
from jax.experimental import pallas as pl
from jax.experimental.pallas import tpu as pltpu
from jax.sharding import PartitionSpec as P

HD = 128

moment_decay = 0.8
square_decay = 0.9
square_floor = 1.0
norm_floor = 0.01
step_rate = 0.01

BF = jnp.bfloat16
F32 = jnp.float32
MESH = pl.DeviceIdType.MESH


def exchange_kernel(
    fs,
    tp,
    x_hbm,
    qc_hbm,
    kc_hbm,
    qm_hbm,
    km_hbm,
    qb_hbm,
    kb_hbm,
    qf_ref,
    qs_ref,
    kf_ref,
    ks_ref,
    qfn_ref,
    qsn_ref,
    kfn_ref,
    ksn_ref,
    ratio_ref,
    sums_ref,
    gathered,
    basis_out,
    basis,
    x_v,
    cot,
    master,
    rounded,
    half_send,
    half_recv,
    half_own,
    z_send,
    z_recv,
    low,
    proj,
    proj_send,
    proj_recv,
    load_sem,
    b_send,
    b_recv,
    d_send,
    d_recv,
    p_send,
    p_recv,
    zr_send,
    zr_recv,
    zg_send,
    zg_recv,
    pf_send,
    pf_recv,
    rs_send,
    rs_recv,
    ag_send,
    ag_recv,
    m_send,
    m_recv,
    out_sem,
):
    f = lax.axis_index("fs")
    t = lax.axis_index("tp")
    z, c = t // 2, t % 2
    depth = tp // 2
    relay = fs == 4
    rows, rank = qb_hbm.shape
    width = qc_hbm.shape[1]
    tokens, columns = x_v.shape
    part = rank // fs
    half_rows = rows // 2
    half = tokens // 2
    chunk = tokens // tp

    def at(start, size):
        return pl.ds(pl.multiple_of(start, size), size)

    def remote(src, dst, send, recv, df, dt):
        return pltpu.make_async_remote_copy(
            src_ref=src,
            dst_ref=dst,
            send_sem=send,
            recv_sem=recv,
            device_id=(df, dt),
            device_id_type=MESH,
        )

    loads = [
        pltpu.make_async_copy(qb_hbm, basis.at[0, at(f * rows, rows)], load_sem.at[0]),
        pltpu.make_async_copy(kb_hbm, basis.at[1, at(f * rows, rows)], load_sem.at[1]),
        pltpu.make_async_copy(qm_hbm, master.at[0], load_sem.at[2]),
        pltpu.make_async_copy(km_hbm, master.at[1], load_sem.at[3]),
        pltpu.make_async_copy(x_hbm, x_v, load_sem.at[4]),
        pltpu.make_async_copy(qc_hbm, cot.at[0], load_sem.at[5]),
        pltpu.make_async_copy(kc_hbm, cot.at[1], load_sem.at[6]),
    ]
    for load in loads:
        load.start()

    barrier = pltpu.get_barrier_semaphore()
    for m in range(1, fs):
        pl.semaphore_signal(barrier, inc=1, device_id=(f ^ m, t), device_id_type=MESH)
    pl.semaphore_signal(barrier, inc=1, device_id=(f, t ^ 1), device_id_type=MESH)
    for d in range(1, depth):
        other = lax.rem(z + d, depth) * 2 + c
        pl.semaphore_signal(barrier, inc=1, device_id=(f, other), device_id_type=MESH)
    loads[0].wait()
    loads[1].wait()
    pl.semaphore_wait(barrier, fs - 1 + depth)

    def basis_copy(j, m, owner, target):
        piece = basis.at[j, at(owner * rows + c * half_rows, half_rows)]
        return remote(piece, piece, b_send.at[m, j], b_recv.at[m, j], target, t)

    direct = [m for m in range(1, fs) if not (relay and m == 3)]
    basis_copies = {}
    for m in direct:
        for j in (0, 1) if m % 2 else (1, 0):
            basis_copies[m, j] = basis_copy(j, m, f, f ^ m)
            basis_copies[m, j].start()

    loads[2].wait()
    loads[3].wait()
    tile = min(rows, 128)

    for j in range(2):

        @pl.loop(0, rows // tile)
        def _(i, j=j):
            place = at(i * tile, tile)
            rounded[j, place, :] = master[j, place, :].astype(BF)

    def master_copy(j, m):
        return remote(
            rounded.at[j],
            gathered.at[j, at(f * rows, rows)],
            m_send.at[m, j],
            m_recv.at[m, j],
            f ^ m,
            t,
        )

    def master_relay(j, source, target):
        piece = gathered.at[j, at((f ^ source) * rows, rows)]
        return remote(piece, piece, m_send.at[3, j], m_recv.at[3, j], f ^ target, t)

    if relay:
        basis_copies[1, 0].wait_recv()
        basis_copies[3, 0] = basis_copy(0, 3, f ^ 1, f ^ 2)
        basis_copies[3, 0].start()
        basis_copies[2, 1].wait_recv()
        basis_copies[3, 1] = basis_copy(1, 3, f ^ 2, f ^ 1)
        basis_copies[3, 1].start()

    master_copies = {}
    first_masters = [(1, 0), (2, 1)] if relay else [(m, 0) for m in direct]
    for m, j in first_masters:
        master_copies[m, j] = master_copy(j, m)
        master_copies[m, j].start()

    waited = {(1, 0), (2, 1)} if relay else set()
    for m in range(1, fs):
        for j in range(2):
            if (m, j) not in waited:
                basis_copies[m, j].wait_recv()

    partner_copies = []
    for m in range(1, fs):
        piece = basis.at[:, at((f ^ m) * rows + c * half_rows, half_rows)]
        copy = remote(piece, piece, d_send.at[m], d_recv.at[m], f, t ^ 1)
        copy.start()
        partner_copies.append(copy)

    loads[4].wait()
    step = min(half, 256)

    def project(start, j):
        return jnp.dot(
            x_v[at(start, step), :],
            basis[j, at(t * columns, columns), :],
            preferred_element_type=F32,
        )

    for j in range(2):

        @pl.loop(0, half // step)
        def _(i, j=j):
            half_send[at(i * step, step), j * rank : (j + 1) * rank] = project(
                (1 - c) * half + i * step, j
            ).astype(BF)

    swap = remote(half_send, half_recv, p_send, p_recv, f, t ^ 1)
    swap.start()
    for j in range(2):

        @pl.loop(0, half // step)
        def _(i, j=j):
            half_own[at(i * step, step), j * rank : (j + 1) * rank] = project(
                c * half + i * step, j
            )

    swap.wait_recv()

    @pl.loop(0, half // chunk)
    def _(i):
        place = at(i * chunk, chunk)
        both = half_own[place, :] + half_recv[place, :].astype(F32)
        half_own[place, :] = both
        z_send[place, :] = both.astype(BF)

    z_copies = []
    for d in range(1, depth):
        other = lax.rem(z + d, depth)
        copy = remote(
            z_send.at[at(other * chunk, chunk)],
            z_recv.at[d],
            zr_send.at[d],
            zr_recv.at[d],
            f,
            other * 2 + c,
        )
        copy.start()
        z_copies.append(copy)
    total = half_own[at(z * chunk, chunk), :]
    for d in range(1, depth):
        z_copies[d - 1].wait_recv()
        total = total + z_recv[d].astype(F32)
    low[at(c * half + z * chunk, chunk), :] = total.astype(BF)

    def low_piece(d, core):
        return low.at[at(core * half + lax.rem(z + depth - d, depth) * chunk, chunk)]

    g_copies = []
    for d in range(1, depth):
        other = lax.rem(z + d, depth)
        copy = remote(
            low_piece(0, c), low_piece(0, c), zg_send.at[d], zg_recv.at[d], f, other * 2 + c
        )
        copy.start()
        g_copies.append(copy)
    forwards = []
    for d in range(depth):
        if d > 0:
            g_copies[d - 1].wait_recv()
        copy = remote(low_piece(d, c), low_piece(d, c), pf_send.at[d], pf_recv.at[d], f, t ^ 1)
        copy.start()
        forwards.append(copy)
    loads[5].wait()
    loads[6].wait()
    for copy in forwards:
        copy.wait_recv()

    for j in range(2):
        product = lax.dot_general(
            low[:, j * rank : (j + 1) * rank],
            cot[j],
            (((0,), (0,)), ((), ())),
            preferred_element_type=F32,
        )
        proj[j] = product
        proj_send[j] = product.astype(BF)
    r_copies = []
    for m in range(1, fs):
        copy = remote(
            proj_send.at[:, at((f ^ m) * part, part)],
            proj_recv.at[m],
            rs_send.at[m],
            rs_recv.at[m],
            f ^ m,
            t,
        )
        copy.start()
        r_copies.append(copy)
    for copy in r_copies:
        copy.wait_recv()

    own = at(f * part, part)
    moments = ((qf_ref, qs_ref, qfn_ref, qsn_ref), (kf_ref, ks_ref, kfn_ref, ksn_ref))
    for j, (first, second, first_out, second_out) in enumerate(moments):
        summed = proj[j, own, :]
        for m in range(1, fs):
            summed = summed + proj_recv[m, j].astype(F32)
        first_new = moment_decay * first[...] + (1.0 - moment_decay) * summed
        second_new = square_decay * second[...] + (1.0 - square_decay) * summed * summed
        first_out[...] = first_new
        second_out[...] = second_new
        ratio_ref[j, own, :] = (first_new / jnp.sqrt(second_new + square_floor)).astype(BF)

    a_copies = []
    for m in range(1, fs):
        piece = ratio_ref.at[:, own]
        copy = remote(piece, piece, ag_send.at[m], ag_recv.at[m], f ^ m, t)
        copy.start()
        a_copies.append(copy)

    for m in direct:
        for j in range(2):
            if (m, j) not in master_copies:
                master_copies[m, j] = master_copy(j, m)
                master_copies[m, j].start()
    if relay:
        master_copies[1, 0].wait_recv()
        master_copies[3, 0] = master_relay(0, 1, 2)
        master_copies[3, 0].start()
        master_copies[2, 1].wait_recv()
        master_copies[3, 1] = master_relay(1, 2, 1)
        master_copies[3, 1].start()

    for copy in partner_copies:
        copy.wait_recv()
    store = pltpu.make_async_copy(basis, basis_out, out_sem)
    store.start()
    for copy in a_copies:
        copy.wait_recv()

    high = min(rows, 256)
    for j in range(2):

        def add(i, total, j=j):
            update = jnp.dot(
                basis[j, at(i * high, high), :], ratio_ref[j], preferred_element_type=F32
            )
            return total + jnp.sum((update * update).reshape(high // 8, 8, width), axis=0)

        sums_ref[j] = lax.fori_loop(0, fs * rows // high, add, jnp.zeros((8, width), F32))

    store.wait()
    early = {(1, 0), (2, 1)} if relay else set()
    for m in range(1, fs):
        for j in range(2):
            if (m, j) not in early:
                master_copies[m, j].wait_recv()
    for copy in list(basis_copies.values()) + partner_copies + [swap] + z_copies:
        copy.wait_send()
    for copy in g_copies + forwards + r_copies + a_copies + list(master_copies.values()):
        copy.wait_send()


def final_kernel(
    own_steps,
    fs_ref,
    sums_ref,
    ratio_ref,
    basis_ref,
    gathered_ref,
    qm_ref,
    km_ref,
    qstep_ref,
    qweight_ref,
    qcopy_ref,
    kstep_ref,
    kweight_ref,
    kcopy_ref,
    *,
    count,
):
    i = pl.program_id(0)
    outs = ((qm_ref, qstep_ref, qweight_ref, qcopy_ref), (km_ref, kstep_ref, kweight_ref, kcopy_ref))
    for j, (master, step_out, weight_out, copy_out) in enumerate(outs):
        sums = jnp.sum(sums_ref[j], axis=0, keepdims=True)
        heads = []
        for h in range(sums.shape[1] // HD):
            total = jnp.sum(sums[:, h * HD : (h + 1) * HD], axis=1, keepdims=True)
            scale = 1.0 / jnp.sqrt(total / (count * HD) + norm_floor)
            heads.append(jnp.broadcast_to(scale, (1, HD)))
        scale = jnp.concatenate(heads, axis=1)
        update = jnp.dot(basis_ref[j], ratio_ref[j], preferred_element_type=F32)
        step = update * scale

        @pl.when(i < own_steps)
        def _(master=master, step_out=step_out, weight_out=weight_out, copy_out=copy_out, step=step):
            weight = master[...] - step_rate * step
            step_out[...] = step
            weight_out[...] = weight
            copy_out[...] = weight.astype(BF)

        @pl.when(i >= own_steps)
        def _(j=j, copy_out=copy_out, step=step):
            copy_out[...] = (gathered_ref[j].astype(F32) - step_rate * step).astype(BF)


def body(fs, tp, *args):
    saved_input, query_cot, _, query_master, key_master, query_basis = args[:6]
    rows, rank = query_basis.shape
    tokens, columns = saved_input.shape
    width = query_cot.shape[1]
    part = rank // fs
    depth = tp // 2
    count = fs * rows
    half, chunk = tokens // 2, tokens // tp
    any_spec = pl.BlockSpec(memory_space=pl.ANY)
    vmem = pl.BlockSpec(memory_space=pltpu.VMEM)
    dma = pltpu.SemaphoreType.DMA
    moment = jax.ShapeDtypeStruct((part, width), F32)
    pairs = []
    for shape in ((fs, 2), (fs,), (), (depth,), (depth,), (depth,), (fs,), (fs,), (fs, 2)):
        pairs += [dma(shape), dma(shape)]
    results = pl.pallas_call(
        functools.partial(exchange_kernel, fs, tp),
        name="exchange",
        out_shape=(
            moment,
            moment,
            moment,
            moment,
            jax.ShapeDtypeStruct((2, rank, width), BF),
            jax.ShapeDtypeStruct((2, 8, width), F32),
            jax.ShapeDtypeStruct((2, count, width), BF),
            jax.ShapeDtypeStruct((2, count, rank), BF),
        ),
        in_specs=[any_spec] * 7 + [vmem] * 4,
        out_specs=(vmem,) * 6 + (any_spec,) * 2,
        scratch_shapes=[
            pltpu.VMEM((2, count, rank), BF),
            pltpu.VMEM((tokens, columns), BF),
            pltpu.VMEM((2, tokens, width), BF),
            pltpu.VMEM((2, rows, width), F32),
            pltpu.VMEM((2, rows, width), BF),
            pltpu.VMEM((half, 2 * rank), BF),
            pltpu.VMEM((half, 2 * rank), BF),
            pltpu.VMEM((half, 2 * rank), F32),
            pltpu.VMEM((half, 2 * rank), BF),
            pltpu.VMEM((depth, chunk, 2 * rank), BF),
            pltpu.VMEM((tokens, 2 * rank), BF),
            pltpu.VMEM((2, rank, width), F32),
            pltpu.VMEM((2, rank, width), BF),
            pltpu.VMEM((fs, 2, part, width), BF),
            dma((7,)),
            *pairs,
            dma,
        ],
        compiler_params=pltpu.CompilerParams(
            collective_id=0, has_side_effects=True, vmem_limit_bytes=60 * 1024 * 1024
        ),
    )(*args)
    qfn, qsn, kfn, ksn, ratio, sums, gathered, basis = results

    tile = min(rows, 256)
    own_steps = rows // tile
    steps = count // tile

    def own_row(i, place):
        return (jnp.minimum(i, own_steps - 1), 0)

    def full_row(i, place):
        return (lax.rem(place[0] * own_steps + i, steps), 0)

    def full_pair(i, place):
        return (0, lax.rem(place[0] * own_steps + i, steps), 0)

    def gathered_pair(i, place):
        return (0, lax.rem(place[0] * own_steps + jnp.maximum(i, own_steps), steps), 0)

    def whole(i, place):
        return (0, 0, 0)

    own_spec = pl.BlockSpec((tile, width), own_row)
    full_spec = pl.BlockSpec((tile, width), full_row)
    place = jnp.reshape(lax.axis_index("fs"), (1,)).astype(jnp.int32)
    big = jax.ShapeDtypeStruct((rows, width), F32)
    copied = jax.ShapeDtypeStruct((count, width), BF)
    qstep, qweight, qcopy, kstep, kweight, kcopy = pl.pallas_call(
        functools.partial(final_kernel, own_steps, count=count),
        name="final",
        out_shape=(big, big, copied, big, big, copied),
        grid_spec=pltpu.PrefetchScalarGridSpec(
            num_scalar_prefetch=1,
            grid=(steps,),
            in_specs=[
                pl.BlockSpec((2, 8, width), whole),
                pl.BlockSpec((2, rank, width), whole),
                pl.BlockSpec((2, tile, rank), full_pair),
                pl.BlockSpec((2, tile, width), gathered_pair),
                own_spec,
                own_spec,
            ],
            out_specs=(own_spec, own_spec, full_spec, own_spec, own_spec, full_spec),
        ),
        compiler_params=pltpu.CompilerParams(vmem_limit_bytes=48 * 1024 * 1024),
    )(place, sums, ratio, basis, gathered, query_master, key_master)
    return (qstep, qweight, qcopy, qfn, qsn, kstep, kweight, kcopy, kfn, ksn)


def solution(mesh):
    split, tall, wide = P("fs", "tp"), P("fs", None), P(None, "tp")
    outs = (split, split, wide, split, split)
    return jax.shard_map(
        functools.partial(body, mesh.shape["fs"], mesh.shape["tp"]),
        mesh=mesh,
        in_specs=(split,) * 5 + (tall, tall) + (split,) * 4,
        out_specs=outs + outs,
        check_vma=False,
    )
```

time: 339 us -> 141 us (0.42)
  waiting for transfers between devices: 250 us -> 0 us
  Pallas kernels: 0 us -> 132 us
  local copies, waits for them, and re-layouts: 33.3 us -> 6.03 us
  blocking collectives: 19.1 us -> 0 us
  between operations: 14.2 us -> 0.7 us
  other arithmetic: 12.5 us -> 0 us
  matrix products: 8.61 us -> 0 us
    all_gather x4 -> x0, waiting for transfers between devices: 156 us -> none  [the longest x1 47.9 us: body(): lax.all_gather(key_weight.astype(jnp.bfloat16), 'fs', axis=0, tiled=True)]
    pallas_call x0 -> x2, Pallas kernels: none -> 132 us  [the longest x1 113 us: body(): pl.pallas_call(functools.partial(exchange_kernel, fs, tp), name='exchange...]
    psum x1 -> x0, waiting for transfers between devices: 65.2 us -> none  [body(): summed_low = lax.psum(local_low, 'tp')]
    reduce_scatter x1 -> x0, waiting for transfers between devices: 27.6 us -> none  [body(): lax.psum_scatter(low_rows(jnp.int32(0), lax.axis_size('fs') * low_count),...]
    unnamed x30 -> x20, local copies, waits for them, and re-layouts: 29.4 us -> 6.03 us
    convert_element_type x3 -> x0, other arithmetic: 11.2 us -> none  [the longest x1 4.98 us: body(): query_weight.astype(jnp.bfloat16)]
    all_gather x1 -> x0, blocking collectives: 10.2 us -> none  [body(): piece = lax.all_gather(ratio, 'fs', axis=0, tiled=True)]
    psum x1 -> x0, blocking collectives: 8.9 us -> none  [body(): lax.psum((head_squares(query_update), head_squares(key_update)), 'fs')]
  transfers between devices with their start and end apart: 6 -> 0, of which waited for: 6 -> 0; matrix products, arithmetic and copies ran while one was open for 8% -> 0% of each run, Pallas kernels for 0% -> 0%
where the time goes in v1:
time: 141 us; the launch traced here: 138 us
  Pallas kernels  132 us (94%)
  local copies, waits for them, and re-layouts  6.03 us (4%)
    pallas_call x1, Pallas kernels, body(): pl.pallas_call(functools.partial(exchange_kernel, fs, tp), name='exchange...  113 us
    pallas_call x1, Pallas kernels, body(): pl.pallas_call(functools.partial(final_kernel, own_steps, count=count), n...  18.6 us
    unnamed x20, local copies, waits for them, and re-layouts  6.03 us

profile of v1, /device:TPU:0, one launch (start us, length us, event | category | flops | bytes accessed | tf_op | source)
XLA Modules:
  0.0 138.2 jit_solution(2384534335145622443)
XLA Ops:
  0.7 0.0 copy-start
  0.7 113.0 %exchange.1 = (f32[64,512]{1,0:T(8,128)}, f32[64,512]{1,0:T(8,128)}, f32[64,512]{1,0:T(8,128)}, f32[64,512]{1,0:T(8,128)}, bf16[2,256,512]{2,1,0:T(8,128)(2,1)},...) custom-call(bf16[1024,512]{1,0:T(8,128)(2,1)} %x_hbm.1, ...), custom_call_target="tpu_custom_call" | custom-call | tf_op jit(solution)/shard_map/exchange/pallas_call | solution.py:416
  113.6 0.0 copy-done
  113.6 0.0 copy-start.1
  113.6 1.6 %copy-done.1 = f32[1024,512]{1,0:T(8,128)S(1)} copy-done((f32[1024,512]{1,0:T(8,128)S(1)}, f32[1024,512]{1,0:T(8,128)}, u32[]{:S(2)}) %copy-start.1) | copy-done | bytes 2097176
  115.2 0.0 copy-start.2
  115.2 1.0 copy-done.2
  116.3 0.0 copy-start.3
  116.3 0.8 copy-done.3
  117.0 0.0 copy-start.7
  117.0 0.0 copy-start.6
  117.0 0.0 copy-start.5
  117.0 0.0 copy-start.4
  117.0 18.6 %final.1 = (f32[1024,512]{1,0:T(8,128)}, f32[1024,512]{1,0:T(8,128)}, bf16[4096,512]{1,0:T(8,128)(2,1)}, f32[1024,512]{1,0:T(8,128)}, f32[1024,512]{1,0:T(8,128)}, /*index=5*/bf16[4096,512]{1,0:T(8,128)(2,1)}) custom-call(s32[1]{0:T(128)} %bitcast.fs_ref, f32[2,8,512]{2,1,0:T(8,128)S(1)} %copy-done.3, bf16[2,256,512]{2,1,0:T(8,128)(2,1)S(1)} %copy-done.2, ...), custom_call_target="tpu_custom_call" | custom-call | tf_op jit(solution)/shard_map/final/pallas_call | solution.py:480
  135.6 0.0 copy-done.7
  135.6 0.7 copy.25
  136.3 0.0 copy-done.6
  136.3 0.7 copy.26
  136.9 0.0 copy-done.5
  136.9 0.7 copy.27
  137.6 0.0 copy-done.4
  137.6 0.7 copy.28
Async XLA Ops:
  0.7 113.0 %copy-start = (f32[1024,512]{1,0:T(8,128)S(1)}, f32[1024,512]{1,0:T(8,128)}, u32[]{:S(2)}) copy-start(f32[1024,512]{1,0:T(8,128)} %qm_ref.1) | copy-start | bytes 6291460
  113.6 1.6 %copy-start.1 = (f32[1024,512]{1,0:T(8,128)S(1)}, f32[1024,512]{1,0:T(8,128)}, u32[]{:S(2)}) copy-start(f32[1024,512]{1,0:T(8,128)} %km_ref.1) | copy-start | bytes 6291460
  115.2 1.0 copy-start.2
  116.3 0.8 copy-start.3
  117.0 18.6 %copy-start.7 = (f32[64,512]{1,0:T(8,128)S(1)}, f32[64,512]{1,0:T(8,128)}, u32[]{:S(2)}) copy-start(f32[64,512]{1,0:T(8,128)} %get-tuple-element.51) | copy-start | bytes 393220
  117.0 19.2 %copy-start.6 = (f32[64,512]{1,0:T(8,128)S(1)}, f32[64,512]{1,0:T(8,128)}, u32[]{:S(2)}) copy-start(f32[64,512]{1,0:T(8,128)} %get-tuple-element.52) | copy-start | bytes 393220
  117.0 19.9 %copy-start.5 = (f32[64,512]{1,0:T(8,128)S(1)}, f32[64,512]{1,0:T(8,128)}, u32[]{:S(2)}) copy-start(f32[64,512]{1,0:T(8,128)} %get-tuple-element.56) | copy-start | bytes 393220
  117.0 20.5 %copy-start.4 = (f32[64,512]{1,0:T(8,128)S(1)}, f32[64,512]{1,0:T(8,128)}, u32[]{:S(2)}) copy-start(f32[64,512]{1,0:T(8,128)} %get-tuple-element.57) | copy-start | bytes 393220

commit v2 on v1

--- a/solution.py
+++ b/solution.py
@@ -39,7 +39,7 @@
     kfn_ref,
     ksn_ref,
     ratio_ref,
-    sums_ref,
+    scale_ref,
     gathered,
     basis_out,
     basis,
@@ -158,9 +158,11 @@
             t,
         )
 
-    def master_relay(j, source, target):
-        piece = gathered.at[j, at((f ^ source) * rows, rows)]
-        return remote(piece, piece, m_send.at[3, j], m_recv.at[3, j], f ^ target, t)
+    def master_relay(j, side):
+        source = 1 + j
+        piece = gathered.at[j, at((f ^ source) * rows + side * half_rows, half_rows)]
+        slot = 3 + side
+        return remote(piece, piece, m_send.at[slot, j], m_recv.at[slot, j], f ^ (2 - j), t)
 
     if relay:
         basis_copies[1, 0].wait_recv()
@@ -171,10 +173,13 @@
         basis_copies[3, 1].start()
 
     master_copies = {}
-    first_masters = [(1, 0), (2, 1)] if relay else [(m, 0) for m in direct]
-    for m, j in first_masters:
-        master_copies[m, j] = master_copy(j, m)
-        master_copies[m, j].start()
+    for turn in range(2):
+        for m in direct:
+            j = (m + 1 + turn) % 2
+            master_copies[m, j] = master_copy(j, m)
+            master_copies[m, j].start()
+    kept = pltpu.make_async_copy(rounded, gathered.at[:, at(f * rows, rows)], out_sem.at[1])
+    kept.start()
 
     waited = {(1, 0), (2, 1)} if relay else set()
     for m in range(1, fs):
@@ -182,13 +187,6 @@
             if (m, j) not in waited:
                 basis_copies[m, j].wait_recv()
 
-    partner_copies = []
-    for m in range(1, fs):
-        piece = basis.at[:, at((f ^ m) * rows + c * half_rows, half_rows)]
-        copy = remote(piece, piece, d_send.at[m], d_recv.at[m], f, t ^ 1)
-        copy.start()
-        partner_copies.append(copy)
-
     loads[4].wait()
     step = min(half, 256)
 
@@ -218,6 +216,13 @@
             )
 
     swap.wait_recv()
+
+    partner_copies = []
+    for m in range(1, fs):
+        piece = basis.at[:, at((f ^ m) * rows + c * half_rows, half_rows)]
+        copy = remote(piece, piece, d_send.at[m], d_recv.at[m], f, t ^ 1)
+        copy.start()
+        partner_copies.append(copy)
 
     @pl.loop(0, half // chunk)
     def _(i):
@@ -289,6 +294,11 @@
         )
         copy.start()
         r_copies.append(copy)
+    if relay:
+        for j in range(2):
+            master_copies[1 + j, j].wait_recv()
+            master_copies[3, j] = master_relay(j, 0)
+            master_copies[3, j].start()
     for copy in r_copies:
         copy.wait_recv()
 
@@ -311,22 +321,14 @@
         copy.start()
         a_copies.append(copy)
 
-    for m in direct:
+    if relay:
         for j in range(2):
-            if (m, j) not in master_copies:
-                master_copies[m, j] = master_copy(j, m)
-                master_copies[m, j].start()
-    if relay:
-        master_copies[1, 0].wait_recv()
-        master_copies[3, 0] = master_relay(0, 1, 2)
-        master_copies[3, 0].start()
-        master_copies[2, 1].wait_recv()
-        master_copies[3, 1] = master_relay(1, 2, 1)
-        master_copies[3, 1].start()
+            master_copies[4, j] = master_relay(j, 1)
+            master_copies[4, j].start()
 
     for copy in partner_copies:
         copy.wait_recv()
-    store = pltpu.make_async_copy(basis, basis_out, out_sem)
+    store = pltpu.make_async_copy(basis, basis_out, out_sem.at[0])
     store.start()
     for copy in a_copies:
         copy.wait_recv()
@@ -340,65 +342,49 @@
             )
             return total + jnp.sum((update * update).reshape(high // 8, 8, width), axis=0)
 
-        sums_ref[j] = lax.fori_loop(0, fs * rows // high, add, jnp.zeros((8, width), F32))
+        sums = lax.fori_loop(0, fs * rows // high, add, jnp.zeros((8, width), F32))
+        sums = jnp.sum(sums, axis=0, keepdims=True)
+        for h in range(width // HD):
+            head = slice(h * HD, (h + 1) * HD)
+            total = jnp.sum(sums[:, head], axis=1, keepdims=True)
+            scale = 1.0 / jnp.sqrt(total / (fs * rows * HD) + norm_floor)
+            scale_ref[j, :, head] = jnp.broadcast_to(scale, (8, HD))
 
     store.wait()
+    kept.wait()
     early = {(1, 0), (2, 1)} if relay else set()
-    for m in range(1, fs):
-        for j in range(2):
-            if (m, j) not in early:
-                master_copies[m, j].wait_recv()
+    for place, copy in master_copies.items():
+        if place not in early:
+            copy.wait_recv()
     for copy in list(basis_copies.values()) + partner_copies + [swap] + z_copies:
         copy.wait_send()
     for copy in g_copies + forwards + r_copies + a_copies + list(master_copies.values()):
         copy.wait_send()
 
 
-def final_kernel(
-    own_steps,
-    fs_ref,
-    sums_ref,
-    ratio_ref,
-    basis_ref,
-    gathered_ref,
-    qm_ref,
-    km_ref,
-    qstep_ref,
-    qweight_ref,
-    qcopy_ref,
-    kstep_ref,
-    kweight_ref,
-    kcopy_ref,
-    *,
-    count,
-):
-    i = pl.program_id(0)
-    outs = ((qm_ref, qstep_ref, qweight_ref, qcopy_ref), (km_ref, kstep_ref, kweight_ref, kcopy_ref))
-    for j, (master, step_out, weight_out, copy_out) in enumerate(outs):
-        sums = jnp.sum(sums_ref[j], axis=0, keepdims=True)
-        heads = []
-        for h in range(sums.shape[1] // HD):
-            total = jnp.sum(sums[:, h * HD : (h + 1) * HD], axis=1, keepdims=True)
-            scale = 1.0 / jnp.sqrt(total / (count * HD) + norm_floor)
-            heads.append(jnp.broadcast_to(scale, (1, HD)))
-        scale = jnp.concatenate(heads, axis=1)
+def final_kernel(*refs):
+    scale_ref, ratio_ref, basis_ref, gathered_ref = refs[:4]
+    inputs, moments, outs, moments_out = refs[4:8], refs[8:12], refs[12:18], refs[18:]
+    for j in range(2):
+        scale = scale_ref[j, 0:1, :]
+        own_basis, master = inputs[2 * j : 2 * j + 2]
+        step_out, weight_out, copy_out = outs[3 * j : 3 * j + 3]
+        update = jnp.dot(own_basis[...], ratio_ref[j], preferred_element_type=F32)
+        step = update * scale
+        step_out[...] = step
+        weight_out[...] = master[...] - step_rate * step
         update = jnp.dot(basis_ref[j], ratio_ref[j], preferred_element_type=F32)
         step = update * scale
-
-        @pl.when(i < own_steps)
-        def _(master=master, step_out=step_out, weight_out=weight_out, copy_out=copy_out, step=step):
-            weight = master[...] - step_rate * step
-            step_out[...] = step
-            weight_out[...] = weight
-            copy_out[...] = weight.astype(BF)
-
-        @pl.when(i >= own_steps)
-        def _(j=j, copy_out=copy_out, step=step):
-            copy_out[...] = (gathered_ref[j].astype(F32) - step_rate * step).astype(BF)
+        copy_out[...] = (gathered_ref[j].astype(F32) - step_rate * step).astype(BF)
+
+    @pl.when(pl.program_id(0) == 0)
+    def _():
+        for source, target in zip(moments, moments_out):
+            target[...] = source[...]
 
 
 def body(fs, tp, *args):
-    saved_input, query_cot, _, query_master, key_master, query_basis = args[:6]
+    saved_input, query_cot, _, query_master, key_master, query_basis, key_basis = args[:7]
     rows, rank = query_basis.shape
     tokens, columns = saved_input.shape
     width = query_cot.shape[1]
@@ -411,7 +397,7 @@
     dma = pltpu.SemaphoreType.DMA
     moment = jax.ShapeDtypeStruct((part, width), F32)
     pairs = []
-    for shape in ((fs, 2), (fs,), (), (depth,), (depth,), (depth,), (fs,), (fs,), (fs, 2)):
+    for shape in ((fs, 2), (fs,), (), (depth,), (depth,), (depth,), (fs,), (fs,), (fs + 1, 2)):
         pairs += [dma(shape), dma(shape)]
     results = pl.pallas_call(
         functools.partial(exchange_kernel, fs, tp),
@@ -445,58 +431,52 @@
             pltpu.VMEM((fs, 2, part, width), BF),
             dma((7,)),
             *pairs,
-            dma,
+            dma((2,)),
         ],
         compiler_params=pltpu.CompilerParams(
             collective_id=0, has_side_effects=True, vmem_limit_bytes=60 * 1024 * 1024
         ),
     )(*args)
-    qfn, qsn, kfn, ksn, ratio, sums, gathered, basis = results
-
-    tile = min(rows, 256)
-    own_steps = rows // tile
-    steps = count // tile
-
-    def own_row(i, place):
-        return (jnp.minimum(i, own_steps - 1), 0)
-
-    def full_row(i, place):
-        return (lax.rem(place[0] * own_steps + i, steps), 0)
-
-    def full_pair(i, place):
-        return (0, lax.rem(place[0] * own_steps + i, steps), 0)
-
-    def gathered_pair(i, place):
-        return (0, lax.rem(place[0] * own_steps + jnp.maximum(i, own_steps), steps), 0)
-
-    def whole(i, place):
+    moments, (ratio, scale, gathered, basis) = results[:4], results[4:]
+
+    steps = min(8, rows // 16)
+    own_tile, tile = rows // steps, count // steps
+
+    def row(i):
+        return (i, 0)
+
+    def pair(i):
+        return (0, i, 0)
+
+    def whole(i):
         return (0, 0, 0)
 
-    own_spec = pl.BlockSpec((tile, width), own_row)
-    full_spec = pl.BlockSpec((tile, width), full_row)
-    place = jnp.reshape(lax.axis_index("fs"), (1,)).astype(jnp.int32)
+    own_spec = pl.BlockSpec((own_tile, width), row)
+    full_spec = pl.BlockSpec((tile, width), row)
+    basis_spec = pl.BlockSpec((own_tile, rank), row)
+    moment_spec = pl.BlockSpec((part, width), lambda i: (0, 0))
     big = jax.ShapeDtypeStruct((rows, width), F32)
     copied = jax.ShapeDtypeStruct((count, width), BF)
-    qstep, qweight, qcopy, kstep, kweight, kcopy = pl.pallas_call(
-        functools.partial(final_kernel, own_steps, count=count),
+    outs = pl.pallas_call(
+        final_kernel,
         name="final",
-        out_shape=(big, big, copied, big, big, copied),
-        grid_spec=pltpu.PrefetchScalarGridSpec(
-            num_scalar_prefetch=1,
-            grid=(steps,),
-            in_specs=[
-                pl.BlockSpec((2, 8, width), whole),
-                pl.BlockSpec((2, rank, width), whole),
-                pl.BlockSpec((2, tile, rank), full_pair),
-                pl.BlockSpec((2, tile, width), gathered_pair),
-                own_spec,
-                own_spec,
-            ],
-            out_specs=(own_spec, own_spec, full_spec, own_spec, own_spec, full_spec),
-        ),
-        compiler_params=pltpu.CompilerParams(vmem_limit_bytes=48 * 1024 * 1024),
-    )(place, sums, ratio, basis, gathered, query_master, key_master)
-    return (qstep, qweight, qcopy, qfn, qsn, kstep, kweight, kcopy, kfn, ksn)
+        out_shape=(big, big, copied) * 2 + (moment,) * 4,
+        grid=(steps,),
+        in_specs=[
+            pl.BlockSpec((2, 8, width), whole),
+            pl.BlockSpec((2, rank, width), whole),
+            pl.BlockSpec((2, tile, rank), pair),
+            pl.BlockSpec((2, tile, width), pair),
+            basis_spec,
+            own_spec,
+            basis_spec,
+            own_spec,
+        ]
+        + [moment_spec] * 4,
+        out_specs=(own_spec, own_spec, full_spec) * 2 + (moment_spec,) * 4,
+        compiler_params=pltpu.CompilerParams(vmem_limit_bytes=60 * 1024 * 1024),
+    )(scale, ratio, basis, gathered, query_basis, query_master, key_basis, key_master, *moments)
+    return (*outs[:3], *outs[6:8], *outs[3:6], *outs[8:])
 
 
 def solution(mesh):

time: 141 us -> 122 us (0.87); the launches traced: 138 us -> 122 us
  Pallas kernels: 132 us -> 121 us
  local copies, waits for them, and re-layouts: 6.03 us -> 0 us
    pallas_call x1, Pallas kernels: 113 us -> 106 us  [body(): pl.pallas_call(functools.partial(exchange_kernel, fs, tp), name='exchange...]
    unnamed x20 -> x0, local copies, waits for them, and re-layouts: 6.03 us -> none
    pallas_call x1, Pallas kernels: 18.6 us -> 15.6 us  [body(): pl.pallas_call(final_kernel, name='final', out_shape=(big, big, copied) *...]
where the time goes in v2:
time: 122 us
  Pallas kernels  121 us (99%)
    pallas_call x1, Pallas kernels, body(): pl.pallas_call(functools.partial(exchange_kernel, fs, tp), name='exchange...  106 us
    pallas_call x1, Pallas kernels, body(): pl.pallas_call(final_kernel, name='final', out_shape=(big, big, copied) *...  15.6 us

profile of v2, /device:TPU:0, one launch (start us, length us, event | category | flops | bytes accessed | tf_op | source)
XLA Modules:
  0.0 122.0 jit_solution(10342961896515980029)
XLA Ops:
  0.6 105.7 %exchange.1 = (f32[64,512]{1,0:T(8,128)}, f32[64,512]{1,0:T(8,128)}, f32[64,512]{1,0:T(8,128)}, f32[64,512]{1,0:T(8,128)}, bf16[2,256,512]{2,1,0:T(8,128)(2,1)},...) custom-call(bf16[1024,512]{1,0:T(8,128)(2,1)} %x_hbm.1, ...), custom_call_target="tpu_custom_call" | custom-call | tf_op jit(solution)/shard_map/exchange/pallas_call | solution.py:402
  106.3 15.6 %final.1 = (f32[1024,512]{1,0:T(8,128)}, f32[1024,512]{1,0:T(8,128)}, bf16[4096,512]{1,0:T(8,128)(2,1)}, f32[1024,512]{1,0:T(8,128)}, f32[1024,512]{1,0:T(8,128)...) custom-call(f32[2,8,512]{2,1,0:T(8,128)} %get-tuple-element.28.refs_, ...), custom_call_target="tpu_custom_call" | custom-call | tf_op jit(solution)/shard_map/final/pallas_call | solution.py:460

commit v3 on v2

--- a/solution.py
+++ b/solution.py
@@ -61,6 +61,8 @@
     b_recv,
     d_send,
     d_recv,
+    zb_send,
+    zb_recv,
     p_send,
     p_recv,
     zr_send,
@@ -135,7 +137,15 @@
     for m in direct:
         for j in (0, 1) if m % 2 else (1, 0):
             basis_copies[m, j] = basis_copy(j, m, f, f ^ m)
-            basis_copies[m, j].start()
+    if relay:
+        basis_copies[3, 0] = basis_copy(0, 3, f ^ 1, f ^ 2)
+        basis_copies[3, 1] = basis_copy(1, 3, f ^ 2, f ^ 1)
+
+    @pl.when(f == z)
+    def _():
+        for m in direct:
+            for j in (0, 1) if m % 2 else (1, 0):
+                basis_copies[m, j].start()
 
     loads[2].wait()
     loads[3].wait()
@@ -165,12 +175,12 @@
         return remote(piece, piece, m_send.at[slot, j], m_recv.at[slot, j], f ^ (2 - j), t)
 
     if relay:
-        basis_copies[1, 0].wait_recv()
-        basis_copies[3, 0] = basis_copy(0, 3, f ^ 1, f ^ 2)
-        basis_copies[3, 0].start()
-        basis_copies[2, 1].wait_recv()
-        basis_copies[3, 1] = basis_copy(1, 3, f ^ 2, f ^ 1)
-        basis_copies[3, 1].start()
+        for j in range(2):
+
+            @pl.when(f ^ (1 + j) == z)
+            def _(j=j):
+                basis_copies[1 + j, j].wait_recv()
+                basis_copies[3, j].start()
 
     master_copies = {}
     for turn in range(2):
@@ -183,9 +193,12 @@
 
     waited = {(1, 0), (2, 1)} if relay else set()
     for m in range(1, fs):
-        for j in range(2):
-            if (m, j) not in waited:
-                basis_copies[m, j].wait_recv()
+
+        @pl.when(f ^ m == z)
+        def _(m=m):
+            for j in range(2):
+                if (m, j) not in waited:
+                    basis_copies[m, j].wait_recv()
 
     loads[4].wait()
     step = min(half, 256)
@@ -216,13 +229,6 @@
             )
 
     swap.wait_recv()
-
-    partner_copies = []
-    for m in range(1, fs):
-        piece = basis.at[:, at((f ^ m) * rows + c * half_rows, half_rows)]
-        copy = remote(piece, piece, d_send.at[m], d_recv.at[m], f, t ^ 1)
-        copy.start()
-        partner_copies.append(copy)
 
     @pl.loop(0, half // chunk)
     def _(i):
@@ -261,6 +267,26 @@
         )
         copy.start()
         g_copies.append(copy)
+
+    def block(d):
+        return lax.rem(z + depth - d, depth)
+
+    def block_piece(d):
+        return basis.at[:, at(block(d) * rows + c * half_rows, half_rows)]
+
+    plane_copies, partner_copies = [], []
+    for d in range(depth):
+        piece = block_piece(d)
+        partner_copies.append(remote(piece, piece, d_send.at[d], d_recv.at[d], f, t ^ 1))
+        piece = block_piece(0)
+        other = lax.rem(z + d, depth) * 2 + c
+        plane_copies.append(remote(piece, piece, zb_send.at[d], zb_recv.at[d], f, other))
+
+    @pl.when(f != z)
+    def _():
+        for copy in plane_copies[1:]:
+            copy.start()
+
     forwards = []
     for d in range(depth):
         if d > 0:
@@ -326,8 +352,20 @@
             master_copies[4, j] = master_relay(j, 1)
             master_copies[4, j].start()
 
-    for copy in partner_copies:
-        copy.wait_recv()
+    for d in range(depth):
+
+        @pl.when(block(d) != f)
+        def _(d=d):
+            if d > 0:
+                plane_copies[d].wait_recv()
+            partner_copies[d].start()
+
+    for d in range(depth):
+
+        @pl.when(block(d) != f)
+        def _(d=d):
+            partner_copies[d].wait_recv()
+
     store = pltpu.make_async_copy(basis, basis_out, out_sem.at[0])
     store.start()
     for copy in a_copies:
@@ -356,7 +394,31 @@
     for place, copy in master_copies.items():
         if place not in early:
             copy.wait_recv()
-    for copy in list(basis_copies.values()) + partner_copies + [swap] + z_copies:
+    for d in range(depth):
+
+        @pl.when(block(d) != f)
+        def _(d=d):
+            partner_copies[d].wait_send()
+
+    @pl.when(f != z)
+    def _():
+        for copy in plane_copies[1:]:
+            copy.wait_send()
+
+    @pl.when(f == z)
+    def _():
+        for m in direct:
+            for j in range(2):
+                basis_copies[m, j].wait_send()
+
+    if relay:
+        for j in range(2):
+
+            @pl.when(f ^ (1 + j) == z)
+            def _(j=j):
+                basis_copies[3, j].wait_send()
+
+    for copy in [swap] + z_copies:
         copy.wait_send()
     for copy in g_copies + forwards + r_copies + a_copies + list(master_copies.values()):
         copy.wait_send()
@@ -397,7 +459,7 @@
     dma = pltpu.SemaphoreType.DMA
     moment = jax.ShapeDtypeStruct((part, width), F32)
     pairs = []
-    for shape in ((fs, 2), (fs,), (), (depth,), (depth,), (depth,), (fs,), (fs,), (fs + 1, 2)):
+    for shape in ((fs, 2), (depth,), (depth,), (), (depth,), (depth,), (depth,), (fs,), (fs,), (fs + 1, 2)):
         pairs += [dma(shape), dma(shape)]
     results = pl.pallas_call(
         functools.partial(exchange_kernel, fs, tp),

time: 122 us -> 125 us (1.025)
  Pallas kernels: 121 us -> 123 us
    pallas_call x1, Pallas kernels: 106 us -> 108 us  [body(): pl.pallas_call(functools.partial(exchange_kernel, fs, tp), name='exchange...]
where the time goes in v3:
time: 125 us; the launch traced here: 124 us
  Pallas kernels  123 us (98%)
    pallas_call x1, Pallas kernels, body(): pl.pallas_call(functools.partial(exchange_kernel, fs, tp), name='exchange...  108 us
    pallas_call x1, Pallas kernels, body(): pl.pallas_call(final_kernel, name='final', out_shape=(big, big, copied) *...  15.6 us

profile of v3, /device:TPU:0, one launch (start us, length us, event | category | flops | bytes accessed | tf_op | source)
XLA Modules:
  0.0 124.0 jit_solution(14086131389390849732)
XLA Ops:
  0.6 107.8 %exchange.1 = (f32[64,512]{1,0:T(8,128)}, f32[64,512]{1,0:T(8,128)}, f32[64,512]{1,0:T(8,128)}, f32[64,512]{1,0:T(8,128)}, bf16[2,256,512]{2,1,0:T(8,128)(2,1)},...) custom-call(bf16[1024,512]{1,0:T(8,128)(2,1)} %x_hbm.1, ...), custom_call_target="tpu_custom_call" | custom-call | tf_op jit(solution)/shard_map/exchange/pallas_call | solution.py:464
  108.4 15.6 %final.1 = (f32[1024,512]{1,0:T(8,128)}, f32[1024,512]{1,0:T(8,128)}, bf16[4096,512]{1,0:T(8,128)(2,1)}, f32[1024,512]{1,0:T(8,128)}, f32[1024,512]{1,0:T(8,128)...) custom-call(f32[2,8,512]{2,1,0:T(8,128)} %get-tuple-element.28.refs_, ...), custom_call_target="tpu_custom_call" | custom-call | tf_op jit(solution)/shard_map/final/pallas_call | solution.py:522
